TPU v7x, 32 devices: a whole 2x2x4 slice. The times are simulated.
32 devices in a mesh: fs: 4 (over y, x), tp: 8 (over z, core).
Axes of the slice: x: 2, y: 2, z: 4, core: 2. Of those that a mesh axis runs over, the one named last changes fastest.
Arguments:
- inputs: bfloat16 [8, 320, 2048], P('tp'), may hold values from -6 to 6
- cotangent: bfloat16 [8, 320, 2048], P('tp'), may hold values from -8 to 8
- gate_weight: bfloat16 [2048, 5632], P('tp', 'fs'), may hold values from -0.125 to 0.125
- up_weight: bfloat16 [2048, 5632], P('tp', 'fs'), may hold values from -0.125 to 0.125
- down_weight: bfloat16 [5632, 2048], P('fs', 'tp'), may hold values from -0.078125 to 0.078125
Outputs:
- input_grad: bfloat16 [8, 320, 2048], P('tp')
- down_grad: float32 [5632, 2048], P('fs', 'tp')
All inputs are finite; a program needn't handle non-finite values.
Results may differ from a plain program's by a relative error of at most 0.023.
Values may be sent and summed in bfloat16 or wider, within the bound.
A program may use at most 64 MiB of HBM per device.

v0:
```python
import jax
import jax.numpy as jnp
from jax import lax
from jax.sharding import PartitionSpec as P


def contract_hidden(left, right):
    return lax.dot_general(
        left, right, (((1,), (1,)), ((), ())), preferred_element_type=jnp.float32
    )


def contract_tokens(left, right):
    return lax.dot_general(
        left, right, (((0,), (0,)), ((), ())), preferred_element_type=jnp.float32
    )


def per_device(inputs, cotangent, gate_weight, up_weight, down_weight):
    rows_in = inputs[0]
    rows_grad = cotangent[0]
    token_count = rows_in.shape[0]
    model_width = rows_in.shape[1]
    gate_full, up_full, down_tall = (
        lax.all_gather(gate_weight, "tp", axis=0, tiled=True),
        lax.all_gather(up_weight, "tp", axis=0, tiled=True),
        lax.all_gather(down_weight.T, "tp", axis=0, tiled=True),
    )
    gate_pre = jnp.dot(rows_in, gate_full, preferred_element_type=jnp.float32)
    up_pre = jnp.dot(rows_in, up_full, preferred_element_type=jnp.float32)
    sig = jax.nn.sigmoid(gate_pre)
    hidden = (gate_pre * sig * up_pre).astype(jnp.bfloat16)
    hidden_grad = jnp.dot(rows_grad, down_tall, preferred_element_type=jnp.float32)
    gate_grad = (hidden_grad * up_pre * sig * (1.0 + gate_pre * (1.0 - sig))).astype(jnp.bfloat16)
    up_grad = (hidden_grad * gate_pre * sig).astype(jnp.bfloat16)
    partial_down = contract_tokens(hidden, rows_grad)
    down_grad = lax.psum_scatter(
        partial_down.astype(jnp.bfloat16), "tp", scatter_dimension=1, tiled=True
    ).astype(jnp.float32)
    own_sum = lax.psum_scatter(
        (contract_hidden(gate_grad, gate_full) + contract_hidden(up_grad, up_full)).astype(
            jnp.bfloat16
        ),
        "fs",
        scatter_dimension=0,
        tiled=True,
    )
    whole_grad = lax.all_gather(own_sum, "fs", axis=0, tiled=True)
    input_grad = whole_grad.reshape(1, token_count, model_width)
    return (input_grad, down_grad)


def solution(mesh):
    return jax.shard_map(
        per_device,
        mesh=mesh,
        in_specs=(
            P("tp", None, None),
            P("tp", None, None),
            P("tp", "fs"),
            P("tp", "fs"),
            P("fs", "tp"),
        ),
        out_specs=(P("tp", None, None), P("fs", "tp")),
        check_vma=False,
    )
```

profile of v0, /device:TPU:0, one launch (start us, length us, event | category | flops | bytes accessed | tf_op | source)
XLA Modules:
  0.0 342.6 jit_solution(16475560544088254756)
XLA Ops:
  7.2 0.0 all-gather.9.cloned.1.call-start
  7.2 0.7 all-gather.9.cloned.1.call-update
  7.9 0.0 all-gather.7.cloned.1.call-start
  8.0 0.7 all-gather.7.cloned.1.call-update
  8.7 0.0 all-gather.5.cloned.1.call-start
  8.7 0.7 all-gather.5.cloned.1.call-update
  9.4 0.0 reduce-scatter.3.cloned.1.call-start
  9.5 63.3 %all-gather.9.cloned.1.call-done = bf16[2048,1408]{1,0:T(8,128)(2,1)} async-done(((bf16[256,1408]{1,0:T(8,128)(2,1)}), bf16[2048,1408]{1,0:T(8,128)(2,1)}) %all-gather.9.cloned.1.call-update) | async-done | bytes 5767184 | tf_op jit(solution)/shard_map/all_gather | solution.py:25
  72.8 6.1 %fusion.1 = f32[320,1408]{1,0:T(8,128)} fusion(bf16[2048,1408]{1,0:T(8,128)(2,1)} %all-gather.9.cloned.1.call-done, bf16[1,320,2048]{2,1,0:T(8,128)(2,1)S(1)} %copy-done.3), kind=kOutput, calls=%fused_computation.7 | convolution fusion | flops 1845493760 | bytes 8880128 | tf_op jit(solution)/shard_map/dot_general | solution.py:29
  78.8 54.6 %all-gather.7.cloned.1.call-done = bf16[2048,1408]{1,0:T(8,128)(2,1)} async-done(((bf16[256,1408]{1,0:T(8,128)(2,1)}), bf16[2048,1408]{1,0:T(8,128)(2,1)}) %all-gather.7.cloned.1.call-update) | async-done | bytes 5767184 | tf_op jit(solution)/shard_map/all_gather | solution.py:26
  133.5 6.1 %fusion.3 = f32[320,1408]{1,0:T(8,128)} fusion(bf16[2048,1408]{1,0:T(8,128)(2,1)} %all-gather.7.cloned.1.call-done, bf16[1,320,2048]{2,1,0:T(8,128)(2,1)S(1)} %copy-done.3), kind=kOutput, calls=%fused_computation.9 | convolution fusion | flops 1845493760 | bytes 8880128 | tf_op jit(solution)/shard_map/dot_general | solution.py:30
  139.6 55.0 %all-gather.5.cloned.1.call-done = bf16[2048,1408]{0,1:T(8,128)(2,1)} async-done(((bf16[256,1408]{0,1:T(8,128)(2,1)}), bf16[2048,1408]{0,1:T(8,128)(2,1)}) %all-gather.5.cloned.1.call-update) | async-done | bytes 5767184 | tf_op jit(solution)/shard_map/all_gather | solution.py:27
  194.6 5.0 %fusion.6 = f32[320,1408]{1,0:T(8,128)S(1)} fusion(bf16[2048,1408]{0,1:T(8,128)(2,1)} %all-gather.5.cloned.1.call-done, bf16[1,320,2048]{2,1,0:T(8,128)(2,1)S(1)} %copy-done), kind=kOutput, calls=%fused_computation.12 | convolution fusion | flops 1845493760 | bytes 8880128 | tf_op jit(solution)/shard_map/dot_general | solution.py:33
  199.6 4.1 %fusion.8 = f32[320,2048]{1,0:T(8,128)S(1)} fusion(bf16[2048,1408]{1,0:T(8,128)(2,1)S(1)} %copy-done.2, f32[320,1408]{1,0:T(8,128)S(1)} %copy-done.4, f32[320,1408]{1,0:T(8,128)S(1)} %fusion.6, f32[320,1408]{1,0:T(8,128)} %fusion.3), kind=kOutput, calls=%fused_computation.14 | convolution fusion | flops 1849999360 | bytes 13795328 | tf_op jit(solution)/shard_map/dot_general | solution.py:8
  203.8 3.4 fusion
  207.2 0.0 reduce-scatter.3.cloned.1.call-update
  207.2 0.0 all-gather.11.cloned.1.call-start
  207.3 27.8 %reduce-scatter.3.cloned.1.call-done = bf16[80,2048]{1,0:T(8,128)(2,1)} async-done(((bf16[320,2048]{1,0:T(8,128)(2,1)}), bf16[80,2048]{1,0:T(8,128)(2,1)}) %reduce-scatter.3.cloned.1.call-update) | async-done | bytes 327696 | tf_op jit(solution)/shard_map/reduce_scatter | solution.py:40
  235.1 0.0 reduce-scatter.5.cloned.1.call-start
  235.1 6.7 %convolution_convert_fusion = bf16[1408,2048]{1,0:T(8,128)(2,1)} fusion(bf16[1,320,2048]{2,1,0:T(8,128)(2,1)S(1)} %copy-done, f32[320,1408]{1,0:T(8,128)} %fusion.3, f32[320,1408]{1,0:T(8,128)S(1)} %copy-done.4), kind=kOutput, calls=%fused_computation | convolution fusion | flops 1851080704 | bytes 10682368 | tf_op jit(solution)/shard_map/dot_general | solution.py:14
  241.8 23.6 %all-gather.11.cloned.1.call-done = bf16[320,2048]{1,0:T(8,128)(2,1)} async-done(((bf16[80,2048]{1,0:T(8,128)(2,1)}), bf16[320,2048]{1,0:T(8,128)(2,1)}) %all-gather.11.cloned.1.call-update) | async-done | bytes 1310736 | tf_op jit(solution)/shard_map/all_gather | solution.py:48
  265.4 67.0 %reduce-scatter.5.cloned.1.call-done = bf16[1408,256]{1,0:T(8,128)(2,1)} async-done(((bf16[1408,2048]{1,0:T(8,128)(2,1)}), bf16[1408,256]{1,0:T(8,128)(2,1)}) %reduce-scatter.5.cloned.1.call-update) | async-done | bytes 720912 | tf_op jit(solution)/shard_map/reduce_scatter | solution.py:37
  332.4 2.3 convert_element_type.23
  334.7 1.1 copy.8
  (17 shorter events, 0.1 us)
Async XLA Ops:
  7.2 187.4 %copy-start = (bf16[1,320,2048]{2,1,0:T(8,128)(2,1)S(1)}, bf16[1,320,2048]{2,1,0:T(8,128)(2,1)}, u32[]{:S(2)}) copy-start(bf16[1,320,2048]{2,1,0:T(8,128)(2,1)} %param.6) | copy-start | bytes 3932164
  7.2 65.6 %copy-start.3 = (bf16[1,320,2048]{2,1,0:T(8,128)(2,1)S(1)}, bf16[1,320,2048]{2,1,0:T(8,128)(2,1)}, u32[]{:S(2)}) copy-start(bf16[1,320,2048]{2,1,0:T(8,128)(2,1)} %param.5) | copy-start | bytes 3932164
  7.2 65.6 %all-gather.9.cloned.1.call-start = ((), (), s32[]{:S(2)}) async-start(), calls=%async_computation.4 | async-start | bytes 6488064 | tf_op jit(solution)/shard_map/all_gather | solution.py:25
  7.9 125.5 %all-gather.7.cloned.1.call-start = ((), (), s32[]{:S(2)}) async-start(), calls=%async_computation.3 | async-start | bytes 6488064 | tf_op jit(solution)/shard_map/all_gather | solution.py:26
  8.7 185.9 %all-gather.5.cloned.1.call-start = ((), (), s32[]{:S(2)}) async-start(), calls=%async_computation.2 | async-start | bytes 6488064 | tf_op jit(solution)/shard_map/all_gather | solution.py:27
  9.4 225.6 %reduce-scatter.3.cloned.1.call-start = ((), (), s32[]{:S(2)}) async-start(), calls=%async_computation.5 | async-start | bytes 1638400 | tf_op jit(solution)/shard_map/reduce_scatter | solution.py:40
  139.6 60.1 %copy-start.4 = (f32[320,1408]{1,0:T(8,128)S(1)}, f32[320,1408]{1,0:T(8,128)}, u32[]{:S(2)}) copy-start(f32[320,1408]{1,0:T(8,128)} %fusion.1) | copy-start | bytes 5406724
  194.6 5.0 %copy-start.2 = (bf16[2048,1408]{1,0:T(8,128)(2,1)S(1)}, bf16[2048,1408]{1,0:T(8,128)(2,1)}, u32[]{:S(2)}) copy-start(bf16[2048,1408]{1,0:T(8,128)(2,1)} %all-gather.9.cloned.1.call-done) | copy-start | bytes 17301508
  194.6 9.2 %slice-start = ((s8[5767168]{0:T(1024)(128)(4,1)}), s8[4194304]{0:T(1024)(128)(4,1)S(1)}, s32[]{:S(2)}) async-start(s8[5767168]{0:T(1024)(128)(4,1)} %bitcast.19), calls=%async_computation.8 | async-start | bytes 8388608
  199.6 4.2 %slice-start.1 = ((s8[5767168]{0:T(1024)(128)(4,1)}), s8[1572864]{0:T(1024)(128)(4,1)S(1)}, s32[]{:S(2)}) async-start(s8[5767168]{0:T(1024)(128)(4,1)} %bitcast.19), calls=%async_computation.9 | async-start | bytes 3145728
  207.2 58.2 %all-gather.11.cloned.1.call-start = ((), (), s32[]{:S(2)}) async-start(), calls=%async_computation.6 | async-start | bytes 1638400 | tf_op jit(solution)/shard_map/all_gather | solution.py:48
  235.1 97.3 %reduce-scatter.5.cloned.1.call-start = ((), (), s32[]{:S(2)}) async-start(), calls=%async_computation.7 | async-start | bytes 6488064 | tf_op jit(solution)/shard_map/reduce_scatter | solution.py:37
  265.4 69.3 %copy-start.1 = (bf16[320,2048]{1,0:T(8,128)(2,1)S(1)}, bf16[320,2048]{1,0:T(8,128)(2,1)}, u32[]{:S(2)}) copy-start(bf16[320,2048]{1,0:T(8,128)(2,1)} %all-gather.11.cloned.1.call-done) | copy-start | bytes 3932164
Sparse Core Ops, SparseCore 0:
  9.6 63.0 all-gather.8
  74.4 59.0 all-gather.6
  135.1 59.4 all-gather.4
  207.3 27.6 reduce-scatter.2
  236.7 28.6 all-gather.10
  267.6 64.7 reduce-scatter.4
where the time goes:
time: 343 us
  waiting for transfers between devices  293 us (85%)
  matrix products  31.3 us (9%)
  between operations  14.2 us (4%)
    reduce_scatter x1, waiting for transfers between devices, per_device(): lax.psum_scatter(partial_down.astype(jnp.bfloat16), 'tp', scatter_dimensi...  67 us
    all_gather x1, waiting for transfers between devices, per_device(): lax.all_gather(gate_weight, 'tp', axis=0, tiled=True)  63.3 us
    all_gather x1, waiting for transfers between devices, per_device(): lax.all_gather(down_weight.T, 'tp', axis=0, tiled=True)  55 us
    all_gather x1, waiting for transfers between devices, per_device(): lax.all_gather(up_weight, 'tp', axis=0, tiled=True)  54.6 us
    reduce_scatter x1, waiting for transfers between devices, per_device(): lax.psum_scatter((contract_hidden(gate_grad, gate_full) + contract_hidden...  27.8 us
    all_gather x1, waiting for transfers between devices, per_device(): whole_grad = lax.all_gather(own_sum, 'fs', axis=0, tiled=True)  23.6 us
    dot_general x2, matrix products, contract_hidden(): lax.dot_general(left, right, (((1,), (1,)), ((), ())), preferred_element_...  7.51 us
  transfers between devices with their start and end apart: 6, of which 6 were waited for; matrix products, arithmetic and copies ran while one was open for 5% of the time, Pallas kernels for 0%

commit v1 on v0

--- a/solution.py
+++ b/solution.py
@@ -45,7 +45,12 @@
         scatter_dimension=0,
         tiled=True,
     )
-    whole_grad = lax.all_gather(own_sum, "fs", axis=0, tiled=True)
+    ring = [own_sum]
+    for hop in range(3):
+        ring.append(lax.ppermute(ring[-1], "fs", [(dev, (dev + 1) % 4) for dev in range(4)]))
+    whole_grad = jnp.roll(
+        jnp.concatenate(ring[::-1], axis=0), (lax.axis_index("fs") + 1) * ring[0].shape[0], axis=0
+    )
     input_grad = whole_grad.reshape(1, token_count, model_width)
     return (input_grad, down_grad)
 

time: 343 us -> 311 us (0.907)
  waiting for transfers between devices: 293 us -> 259 us
    reduce_scatter x1, waiting for transfers between devices: 67 us -> 36.9 us  [per_device(): lax.psum_scatter(partial_down.astype(jnp.bfloat16), 'tp', scatter_dimensi...]
    ppermute x0 -> x3, waiting for transfers between devices: none -> 26.3 us  [per_device(): lax.ppermute(ring[-1], 'fs', [(dev, (dev + 1) % 4) for dev in range(4)])]
    all_gather x1 -> x0, waiting for transfers between devices: 23.6 us -> none  [per_device(): whole_grad = lax.all_gather(own_sum, 'fs', axis=0, tiled=True)]
    reduce_scatter x1, waiting for transfers between devices: 27.8 us -> 21.1 us  [per_device(): lax.psum_scatter((contract_hidden(gate_grad, gate_full) + contract_hidden...]
  transfers between devices with their start and end apart: 6 -> 8, of which waited for: 6 -> 8; matrix products, arithmetic and copies ran while one was open for 5% -> 7% of each run, Pallas kernels for 0% -> 0%
where the time goes in v1:
time: 311 us
  waiting for transfers between devices  259 us (83%)
  matrix products  31.3 us (10%)
  between operations  13.9 us (4%)
    all_gather x1, waiting for transfers between devices, per_device(): lax.all_gather(gate_weight, 'tp', axis=0, tiled=True)  63.3 us
    all_gather x1, waiting for transfers between devices, per_device(): lax.all_gather(down_weight.T, 'tp', axis=0, tiled=True)  55 us
    all_gather x1, waiting for transfers between devices, per_device(): lax.all_gather(up_weight, 'tp', axis=0, tiled=True)  54.6 us
    reduce_scatter x1, waiting for transfers between devices, per_device(): lax.psum_scatter(partial_down.astype(jnp.bfloat16), 'tp', scatter_dimensi...  36.9 us
    ppermute x3, waiting for transfers between devices, per_device(): lax.ppermute(ring[-1], 'fs', [(dev, (dev + 1) % 4) for dev in range(4)])  26.3 us
    reduce_scatter x1, waiting for transfers between devices, per_device(): lax.psum_scatter((contract_hidden(gate_grad, gate_full) + contract_hidden...  21.1 us
    dot_general x2, matrix products, contract_hidden(): lax.dot_general(left, right, (((1,), (1,)), ((), ())), preferred_element_...  7.51 us
    dot_general x1, matrix products, contract_tokens(): lax.dot_general(left, right, (((0,), (0,)), ((), ())), preferred_element_...  6.69 us
  transfers between devices with their start and end apart: 8, of which 8 were waited for; matrix products, arithmetic and copies ran while one was open for 7% of the time, Pallas kernels for 0%

profile of v1, /device:TPU:0, one launch (start us, length us, event | category | flops | bytes accessed | tf_op | source)
XLA Modules:
  0.0 310.8 jit_solution(9360966864739439444)
XLA Ops:
  7.2 0.7 all-gather.8.cloned.1.call-update
  8.0 0.7 all-gather.6.cloned.1.call-update
  8.7 0.0 all-gather.4.cloned.1.call-start
  8.7 0.7 all-gather.4.cloned.1.call-update
  9.4 0.0 reduce-scatter.3.cloned.1.call-start
  9.5 63.3 %all-gather.8.cloned.1.call-done = bf16[2048,1408]{1,0:T(8,128)(2,1)} async-done(((bf16[256,1408]{1,0:T(8,128)(2,1)}), bf16[2048,1408]{1,0:T(8,128)(2,1)}) %all-gather.8.cloned.1.call-update) | async-done | bytes 5767184 | tf_op jit(solution)/shard_map/all_gather | solution.py:25
  72.8 6.1 %fusion.1 = f32[320,1408]{1,0:T(8,128)} fusion(bf16[2048,1408]{1,0:T(8,128)(2,1)} %all-gather.8.cloned.1.call-done, bf16[1,320,2048]{2,1,0:T(8,128)(2,1)S(1)} %copy-done.3), kind=kOutput, calls=%fused_computation.7 | convolution fusion | flops 1845493760 | bytes 8880128 | tf_op jit(solution)/shard_map/dot_general | solution.py:29
  78.8 54.6 %all-gather.6.cloned.1.call-done = bf16[2048,1408]{1,0:T(8,128)(2,1)} async-done(((bf16[256,1408]{1,0:T(8,128)(2,1)}), bf16[2048,1408]{1,0:T(8,128)(2,1)}) %all-gather.6.cloned.1.call-update) | async-done | bytes 5767184 | tf_op jit(solution)/shard_map/all_gather | solution.py:26
  133.5 6.1 %fusion.3 = f32[320,1408]{1,0:T(8,128)} fusion(bf16[2048,1408]{1,0:T(8,128)(2,1)} %all-gather.6.cloned.1.call-done, bf16[1,320,2048]{2,1,0:T(8,128)(2,1)S(1)} %copy-done.3), kind=kOutput, calls=%fused_computation.9 | convolution fusion | flops 1845493760 | bytes 8880128 | tf_op jit(solution)/shard_map/dot_general | solution.py:30
  139.6 55.0 %all-gather.4.cloned.1.call-done = bf16[2048,1408]{0,1:T(8,128)(2,1)} async-done(((bf16[256,1408]{0,1:T(8,128)(2,1)}), bf16[2048,1408]{0,1:T(8,128)(2,1)}) %all-gather.4.cloned.1.call-update) | async-done | bytes 5767184 | tf_op jit(solution)/shard_map/all_gather | solution.py:27
  194.6 5.0 %fusion.6 = f32[320,1408]{1,0:T(8,128)S(1)} fusion(bf16[2048,1408]{0,1:T(8,128)(2,1)} %all-gather.4.cloned.1.call-done, bf16[1,320,2048]{2,1,0:T(8,128)(2,1)S(1)} %copy-done), kind=kOutput, calls=%fused_computation.12 | convolution fusion | flops 1845493760 | bytes 8880128 | tf_op jit(solution)/shard_map/dot_general | solution.py:33
  199.6 4.1 %fusion.8 = f32[320,2048]{1,0:T(8,128)S(1)} fusion(bf16[2048,1408]{1,0:T(8,128)(2,1)S(1)} %copy-done.2, f32[320,1408]{1,0:T(8,128)S(1)} %copy-done.4, f32[320,1408]{1,0:T(8,128)S(1)} %fusion.6, f32[320,1408]{1,0:T(8,128)} %fusion.3), kind=kOutput, calls=%fused_computation.15 | convolution fusion | flops 1849999360 | bytes 13795328 | tf_op jit(solution)/shard_map/dot_general | solution.py:8
  203.8 3.4 %fusion = bf16[320,2048]{1,0:T(8,128)(2,1)} fusion(f32[320,2048]{1,0:T(8,128)S(1)} %fusion.8, bf16[2048,1408]{1,0:T(8,128)(2,1)S(1)} %bitcast.20, f32[320,1408]{1,0:T(8,128)S(1)} %fusion.6, f32[320,1408]{1,0:T(8,128)S(1)} %copy-done.4), kind=kOutput, calls=%fused_computation.2 | convolution fusion | flops 1849507840 | bytes 13303808 | tf_op jit(solution)/shard_map/dot_general | solution.py:8
  207.2 0.0 reduce-scatter.5.cloned.1.call-start
  207.3 6.7 %convolution_convert_fusion = bf16[1408,2048]{1,0:T(8,128)(2,1)} fusion(bf16[1,320,2048]{2,1,0:T(8,128)(2,1)S(1)} %copy-done, f32[320,1408]{1,0:T(8,128)} %fusion.3, f32[320,1408]{1,0:T(8,128)S(1)} %copy-done.4), kind=kOutput, calls=%fused_computation | convolution fusion | flops 1851080704 | bytes 10682368 | tf_op jit(solution)/shard_map/dot_general | solution.py:14
  214.0 21.1 %reduce-scatter.3.cloned.1.call-done = bf16[80,2048]{1,0:T(8,128)(2,1)} async-done(((bf16[320,2048]{1,0:T(8,128)(2,1)}), bf16[80,2048]{1,0:T(8,128)(2,1)}) %reduce-scatter.3.cloned.1.call-update) | async-done | bytes 327696 | tf_op jit(solution)/shard_map/reduce_scatter | solution.py:40
  235.0 1.5 collective-permute-start
  236.5 8.9 %collective-permute-done = bf16[80,2048]{1,0:T(8,128)(2,1)S(1)} collective-permute-done((bf16[80,2048]{1,0:T(8,128)(2,1)}, bf16[80,2048]{1,0:T(8,128)(2,1)S(1)}, u32[]{:S(2)}, u32[]{:S(2)}) %collective-permute-start) | collective-permute-done | bytes 327712 | tf_op jit(solution)/shard_map/ppermute | solution.py:50
  245.4 0.6 collective-permute-start.1
  246.0 8.8 %collective-permute-done.1 = bf16[80,2048]{1,0:T(8,128)(2,1)S(1)} collective-permute-done((bf16[80,2048]{1,0:T(8,128)(2,1)S(1)}, bf16[80,2048]{1,0:T(8,128)(2,1)S(1)}, u32[]{:S(2)}, u32[]{:S(2)}) %collective-permute-start.1) | collective-permute-done | bytes 327712 | tf_op jit(solution)/shard_map/ppermute | solution.py:50
  254.8 8.6 %collective-permute-done.2 = bf16[80,2048]{1,0:T(8,128)(2,1)S(1)} collective-permute-done((bf16[80,2048]{1,0:T(8,128)(2,1)S(1)}, bf16[80,2048]{1,0:T(8,128)(2,1)S(1)}, u32[]{:S(2)}, u32[]{:S(2)}) %collective-permute-start.2) | collective-permute-done | bytes 327712 | tf_op jit(solution)/shard_map/ppermute | solution.py:50
  263.6 1.5 dynamic-slice_bitcast_fusion
  265.1 36.9 %reduce-scatter.5.cloned.1.call-done = bf16[1408,256]{1,0:T(8,128)(2,1)} async-done(((bf16[1408,2048]{1,0:T(8,128)(2,1)}), bf16[1408,256]{1,0:T(8,128)(2,1)}) %reduce-scatter.5.cloned.1.call-update) | async-done | bytes 720912 | tf_op jit(solution)/shard_map/reduce_scatter | solution.py:37
  302.0 2.3 convert_element_type.23
  (28 shorter events, 0.3 us)
Async XLA Ops:
  7.2 187.4 %copy-start = (bf16[1,320,2048]{2,1,0:T(8,128)(2,1)S(1)}, bf16[1,320,2048]{2,1,0:T(8,128)(2,1)}, u32[]{:S(2)}) copy-start(bf16[1,320,2048]{2,1,0:T(8,128)(2,1)} %param.6) | copy-start | bytes 3932164
  7.2 65.6 %copy-start.3 = (bf16[1,320,2048]{2,1,0:T(8,128)(2,1)S(1)}, bf16[1,320,2048]{2,1,0:T(8,128)(2,1)}, u32[]{:S(2)}) copy-start(bf16[1,320,2048]{2,1,0:T(8,128)(2,1)} %param.5) | copy-start | bytes 3932164
  7.2 65.6 %all-gather.8.cloned.1.call-start = ((), (), s32[]{:S(2)}) async-start(), calls=%async_computation.4 | async-start | bytes 6488064 | tf_op jit(solution)/shard_map/all_gather | solution.py:25
  7.9 125.5 %all-gather.6.cloned.1.call-start = ((), (), s32[]{:S(2)}) async-start(), calls=%async_computation.3 | async-start | bytes 6488064 | tf_op jit(solution)/shard_map/all_gather | solution.py:26
  8.7 185.9 %all-gather.4.cloned.1.call-start = ((), (), s32[]{:S(2)}) async-start(), calls=%async_computation.2 | async-start | bytes 6488064 | tf_op jit(solution)/shard_map/all_gather | solution.py:27
  9.4 225.6 %reduce-scatter.3.cloned.1.call-start = ((), (), s32[]{:S(2)}) async-start(), calls=%async_computation.5 | async-start | bytes 1638400 | tf_op jit(solution)/shard_map/reduce_scatter | solution.py:40
  139.6 60.1 %copy-start.4 = (f32[320,1408]{1,0:T(8,128)S(1)}, f32[320,1408]{1,0:T(8,128)}, u32[]{:S(2)}) copy-start(f32[320,1408]{1,0:T(8,128)} %fusion.1) | copy-start | bytes 5406724
  194.6 5.0 %copy-start.2 = (bf16[2048,1408]{1,0:T(8,128)(2,1)S(1)}, bf16[2048,1408]{1,0:T(8,128)(2,1)}, u32[]{:S(2)}) copy-start(bf16[2048,1408]{1,0:T(8,128)(2,1)} %all-gather.8.cloned.1.call-done) | copy-start | bytes 17301508
  194.6 9.2 %slice-start = ((s8[5767168]{0:T(1024)(128)(4,1)}), s8[4194304]{0:T(1024)(128)(4,1)S(1)}, s32[]{:S(2)}) async-start(s8[5767168]{0:T(1024)(128)(4,1)} %bitcast.19), calls=%async_computation.7 | async-start | bytes 8388608
  199.6 4.2 %slice-start.1 = ((s8[5767168]{0:T(1024)(128)(4,1)}), s8[1572864]{0:T(1024)(128)(4,1)S(1)}, s32[]{:S(2)}) async-start(s8[5767168]{0:T(1024)(128)(4,1)} %bitcast.19), calls=%async_computation.8 | async-start | bytes 3145728
  207.2 94.8 %reduce-scatter.5.cloned.1.call-start = ((), (), s32[]{:S(2)}) async-start(), calls=%async_computation.6 | async-start | bytes 6488064 | tf_op jit(solution)/shard_map/reduce_scatter | solution.py:37
  235.0 28.4 %copy-start.1 = (bf16[80,2048]{1,0:T(8,128)(2,1)S(1)}, bf16[80,2048]{1,0:T(8,128)(2,1)}, u32[]{:S(2)}) copy-start(bf16[80,2048]{1,0:T(8,128)(2,1)} %reduce-scatter.3.cloned.1.call-done) | copy-start | bytes 983044
  235.0 10.4 %collective-permute-start = (bf16[80,2048]{1,0:T(8,128)(2,1)}, bf16[80,2048]{1,0:T(8,128)(2,1)S(1)}, u32[]{:S(2)}, u32[]{:S(2)}) collective-permute-start(bf16[80,2048]{1,0:T(8,128)(2,1)} %reduce-scatter.3.cloned.1.call-done), channel_id=1, source_target_pairs={{0,8},{8,16},{16,24},{24,0},{1,9},{9,17},{17,25},{25,1},{2,10},{10... | collective-permute-start | bytes 983048 | tf_op jit(solution)/shard_map/ppermute | solution.py:50
  245.4 9.3 %collective-permute-start.1 = (bf16[80,2048]{1,0:T(8,128)(2,1)S(1)}, bf16[80,2048]{1,0:T(8,128)(2,1)S(1)}, u32[]{:S(2)}, u32[]{:S(2)}) collective-permute-start(bf16[80,2048]{1,0:T(8,128)(2,1)S(1)} %collective-permute-done), channel_id=1, source_target_pairs={{0,8},{8,16},{16,24},{24,0},{1,9},{9,17},{17,25},{25,1},{2,10},{10... | collective-permute-start | bytes 983048 | tf_op jit(solution)/shard_map/ppermute | solution.py:50
  254.8 8.6 %collective-permute-start.2 = (bf16[80,2048]{1,0:T(8,128)(2,1)S(1)}, bf16[80,2048]{1,0:T(8,128)(2,1)S(1)}, u32[]{:S(2)}, u32[]{:S(2)}) collective-permute-start(bf16[80,2048]{1,0:T(8,128)(2,1)S(1)} %collective-permute-done.1), channel_id=1, source_target_pairs={{0,8},{8,16},{16,24},{24,0},{1,9},{9,17},{17,25},{25,1},{2,10},{10... | collective-permute-start | bytes 983048 | tf_op jit(solution)/shard_map/ppermute | solution.py:50
Sparse Core Ops, SparseCore 0:
  9.6 63.0 all-gather.7
  74.4 59.0 all-gather.5
  135.1 59.4 all-gather.3
  207.3 27.6 reduce-scatter.2
  237.2 64.7 reduce-scatter.4
